TPU v7x, 32 devices: a whole 2x2x4 slice. The times are simulated.
32 devices in a mesh: dp: 4 (over y, x), kv: 4 (over z), tp: 2 (over core).
Axes of the slice: x: 2, y: 2, z: 4, core: 2. Of those that a mesh axis runs over, the one named last changes fastest.
Arguments:
- tokens: bfloat16 [24, 4096], P('dp', 'kv'), may hold values from -64 to 64
- lengths: int32 [24], P('dp'), may hold values from 128 to 1024, as said below
- attn_gain: float32 [4096], P('kv'), may hold values from 0.1 to 1.9
- query_weight: bfloat16 [4096, 4096], P('kv', 'tp'), may hold values from -0.09375 to 0.09375
- key_weight: bfloat16 [4096, 256], P('kv', 'tp'), may hold values from -0.1875 to 0.1875
- value_weight: bfloat16 [4096, 256], P('kv', 'tp'), may hold values from -0.09375 to 0.09375
- forget_weight: bfloat16 [4096, 4], replicated, may hold values from -0.25 to 0.25
- forget_offset: float32 [4], P('tp'), may hold values from -6 to 0
- cache_keys: bfloat16 [24, 1024, 256], P('dp', 'kv', 'tp'), may hold values from -1600 to 1600
- cache_values: bfloat16 [24, 1024, 256], P('dp', 'kv', 'tp'), may hold values from -6 to 6
- gate_sum: float32 [24, 4, 1024], P('dp', 'tp', 'kv'), may hold values from -82 to 0
- out_weight: bfloat16 [4096, 4096], P('tp', 'kv'), may hold values from -0.1875 to 0.1875
- mlp_gain: float32 [4096], replicated, may hold values from 0.1 to 1.9
- up_weight: bfloat16 [4096, 16384], P(None, ('kv', 'tp')), may hold values from -0.09375 to 0.09375
- down_weight: bfloat16 [16384, 4096], P(('kv', 'tp')), may hold values from -0.0625 to 0.0625
Outputs:
- mixed: bfloat16 [24, 4096], P('dp', ('kv', 'tp'))
Inputs may be any that keep to these rules, and one draw needn't show every extreme that they name: `lengths`: in every draw some sequence has all 1024 positions cached.
All inputs are finite; a program needn't handle non-finite values.
Results may differ from a plain program's by a relative error of at most 0.023.
Values may be sent and summed in bfloat16 or wider, within the bound.
A program may use at most 128 MiB of HBM per device.

v0:
```python
import jax
import jax.numpy as jnp
from jax import lax
from jax.sharding import PartitionSpec as P

D = 4096
HEADS = 64
HD = 64
KEY_VALUE_HEADS = 4


epsilon = 1e-06
floor_score = -1e30


def combined_all(x, axis, combine):
    everything = jax.tree.map(
        lambda part, kind: lax.all_gather(part.astype(kind), axis),
        x,
        (jnp.bfloat16, jnp.bfloat16, jnp.bfloat16),
    )

    def take(k):
        return jax.tree.map(lambda part, own: part[k].astype(own.dtype), everything, x)

    return lax.fori_loop(
        1, lax.axis_size(axis), lambda k, so_far: combine(so_far, take(k)), take(0)
    )


def combine_parts(earlier, later):
    first_top, first_total, first_values = earlier
    second_top, second_total, second_values = later
    merged_top = jnp.maximum(first_top, second_top)
    first_scale = jnp.exp(first_top - merged_top)
    second_scale = jnp.exp(second_top - merged_top)
    first_wide = jnp.repeat(first_scale, HD, axis=1)
    second_wide = jnp.repeat(second_scale, HD, axis=1)
    return (
        merged_top,
        first_total * first_scale + second_total * second_scale,
        first_values * first_wide + second_values * second_wide,
    )


def shards(
    tokens,
    lengths,
    attn_gain,
    query_weight,
    key_weight,
    value_weight,
    forget_weight,
    forget_offset,
    cache_keys,
    cache_values,
    gate_sum,
    out_weight,
    mlp_gain,
    up_weight,
    down_weight,
):
    row_count = tokens.shape[0]
    feature_cols = tokens.shape[1]
    kv_place = lax.axis_index("kv")
    tp_place = lax.axis_index("tp")
    local_heads = key_weight.shape[1] // HD
    group_size = HEADS // KEY_VALUE_HEADS
    token_rows = tokens.astype(jnp.float32)
    scaled_rows = (token_rows * attn_gain[None, :]).astype(jnp.bfloat16)
    square_part = jnp.sum(token_rows * token_rows, axis=1)
    query_part = jnp.dot(scaled_rows, query_weight, preferred_element_type=jnp.float32)
    key_part = jnp.dot(scaled_rows, key_weight, preferred_element_type=jnp.float32)
    value_part = jnp.dot(scaled_rows, value_weight, preferred_element_type=jnp.float32)
    gate_rows = lax.dynamic_slice(
        forget_weight,
        (kv_place * feature_cols, tp_place * local_heads),
        (feature_cols, local_heads),
    )
    forget_part = jnp.dot(scaled_rows, gate_rows, preferred_element_type=jnp.float32)
    query_sum, key_sum, value_sum, forget_sum, square_sum = lax.psum(
        (query_part, key_part, value_part, forget_part, square_part), "kv"
    )
    row_scale = lax.rsqrt(square_sum / D + epsilon)[:, None]
    queries = (query_sum * row_scale).astype(jnp.bfloat16)
    new_key = (key_sum * row_scale).astype(jnp.bfloat16)
    new_value = (value_sum * row_scale).astype(jnp.bfloat16)
    log_forget = jax.nn.log_sigmoid(forget_sum * row_scale + forget_offset[None, :])
    positions_here = cache_keys.shape[1]
    key_heads = cache_keys.reshape(row_count, positions_here, local_heads, HD)
    value_heads = cache_values.reshape(row_count, positions_here, local_heads, HD)
    query_heads = queries.reshape(row_count, local_heads, group_size, HD)
    scores = jnp.einsum(
        "skgd,spkd->skgp", query_heads, key_heads, preferred_element_type=jnp.float32
    ) * HD ** (-0.5)
    scores = scores + gate_sum[:, :, None, :] + log_forget[:, :, None, None]
    cache_pos = kv_place * positions_here + jnp.arange(positions_here)
    active_mask = (cache_pos[None, :] < lengths[:, None])[:, None, None, :]
    local_top = jnp.max(jnp.where(active_mask, scores, floor_score), axis=3)
    weights = jnp.where(active_mask, jnp.exp(scores - local_top[..., None]), 0.0)
    local_total = jnp.sum(weights, axis=3)
    local_values = jnp.einsum(
        "skgp,spkd->skgd",
        weights.astype(jnp.bfloat16),
        value_heads,
        preferred_element_type=jnp.float32,
    )
    head_cols = local_heads * group_size
    merged_top, merged_total, merged_values = combined_all(
        (
            local_top.reshape(row_count, head_cols),
            local_total.reshape(row_count, head_cols),
            local_values.reshape(row_count, head_cols * HD),
        ),
        "kv",
        combine_parts,
    )
    own_score = jnp.einsum(
        "skgd,skd->skg",
        query_heads,
        new_key.reshape(row_count, local_heads, HD),
        preferred_element_type=jnp.float32,
    ).reshape(row_count, head_cols) * HD ** (-0.5)
    final_top = jnp.maximum(merged_top, own_score)
    past_scale = jnp.exp(merged_top - final_top)
    own_weight = jnp.exp(own_score - final_top)
    totals = merged_total * past_scale + own_weight
    own_rounded = lax.optimization_barrier(own_weight.astype(jnp.bfloat16)).astype(jnp.float32)
    own_values = jnp.broadcast_to(
        new_value.astype(jnp.float32).reshape(row_count, local_heads, 1, HD),
        (row_count, local_heads, group_size, HD),
    ).reshape(row_count, head_cols * HD)
    weighted = (
        merged_values * jnp.repeat(past_scale, HD, axis=1)
        + jnp.repeat(own_rounded, HD, axis=1) * own_values
    )
    attended = (weighted / jnp.repeat(totals, HD, axis=1)).astype(jnp.bfloat16)
    partial_out = jnp.dot(attended, out_weight, preferred_element_type=jnp.float32)
    head_sum = lax.psum(partial_out.astype(jnp.bfloat16), "tp").astype(jnp.float32)
    mid_cols = (token_rows + head_sum).astype(jnp.bfloat16)
    mid_rows = lax.all_gather(mid_cols, "kv", axis=1, tiled=True)
    mid_wide = mid_rows.astype(jnp.float32)
    normed_mid = (
        mid_wide
        * mlp_gain[None, :]
        * lax.rsqrt(jnp.mean(mid_wide * mid_wide, axis=1, keepdims=True) + epsilon)
    ).astype(jnp.bfloat16)
    hidden = jnp.square(
        jax.nn.relu(jnp.dot(normed_mid, up_weight, preferred_element_type=jnp.float32))
    ).astype(jnp.bfloat16)
    mixer_term = jnp.dot(hidden, down_weight, preferred_element_type=jnp.float32)
    kv_count = lax.axis_size("kv")
    tp_count = lax.axis_size("tp")
    block_cols = mixer_term.shape[1] // (kv_count * tp_count)
    reordered = (
        mixer_term.reshape(row_count, kv_count, tp_count, block_cols)
        .transpose(0, 2, 1, 3)
        .reshape(row_count, kv_count * tp_count * block_cols)
    )
    pair_share = lax.psum_scatter(
        reordered.astype(jnp.bfloat16), "tp", scatter_dimension=1, tiled=True
    ).astype(jnp.float32)
    mixer_share = lax.psum_scatter(pair_share, "kv", scatter_dimension=1, tiled=True)
    out_cols = mixer_share.shape[1]
    start_col = (kv_place * tp_count + tp_place) * out_cols
    mid_share = lax.dynamic_slice_in_dim(mid_wide, start_col, out_cols, 1)
    return (mid_share + mixer_share).astype(jnp.bfloat16)


def solution(mesh):
    placed = (
        P("dp", "kv"),
        P("dp"),
        P("kv"),
        P("kv", "tp"),
        P("kv", "tp"),
        P("kv", "tp"),
        P(),
        P("tp"),
        P("dp", "kv", "tp"),
        P("dp", "kv", "tp"),
        P("dp", "tp", "kv"),
        P("tp", "kv"),
        P(),
        P(None, ("kv", "tp")),
        P(("kv", "tp"), None),
    )
    return jax.shard_map(
        shards, mesh=mesh, in_specs=placed, out_specs=P("dp", ("kv", "tp")), check_vma=False
    )
```

profile of v0, /device:TPU:0, one launch (start us, length us, event | category | flops | bytes accessed | tf_op | source)
XLA Modules:
  0.0 151.1 jit_solution(10252514063055072850)
XLA Ops:
  6.6 0.9 fusion.20
  7.4 2.9 %fusion.30 = f32[6,2048]{1,0:T(8,128)S(1)} fusion(bf16[1024,2048]{1,0:T(8,128)(2,1)} %param.20, bf16[6,1024]{1,0:T(8,128)(2,1)} %param.17, f32[1024]{0:T(1024)} %param.19), kind=kOutput, calls=%fused_computation.47 | convolution fusion | flops 25184256 | bytes 4259840 | tf_op jit(solution)/shard_map/dot_general | solution.py:72
  10.3 0.9 fusion.24
  11.2 1.1 fusion.26
  12.3 0.9 fusion.28
  13.3 22.1 %all-reduce = (f32[6,2048]{1,0:T(8,128)S(1)}, f32[6]{0:T(128)S(1)}, f32[6,128]{1,0:T(8,128)S(1)}, f32[6,2]{0,1:T(2,128)S(1)}, f32[6,128]{1,0:T(8,128)S(1)}) all-reduce(f32[6,2048]{1,0:T(8,128)S(1)} %fusion.30, f32[6]{0:T(128)S(1)} %fusion.20, f32[6,128]{1,0:T(8,128)S(1)} %fusion.26, ...), channel_id=1, replica_groups=mesh['dp'=4,'kv'=4,'tp'=2] {'kv'}, use_global_device_ids=true, to_apply=%region_0.0 | all-reduce | flops 13842 | bytes 110736 | tf_op jit(solution)/shard_map/psum | solution.py:81
  35.4 0.1 reshape.143
  35.5 0.7 fusion.39
  36.3 0.1 copy.25
  36.4 1.2 copy.24
  37.5 1.2 copy.26
  38.7 0.7 broadcast_compare_fusion
  39.4 1.0 select_reduce_fusion
  40.4 0.2 fusion.8
  40.6 0.3 convolution_convert_fusion.1
  40.9 0.1 convert_element_type.173
  41.0 13.6 %all_gather.17 = bf16[4,6,2048]{2,1,0:T(8,128)(2,1)S(1)} all-gather(bf16[1,6,2048]{2,1,0:T(8,128)(2,1)S(1)} %convert_element_type.173), channel_id=1, replica_groups=mesh['dp'=4,'kv'=4,'tp'=2] {'kv'}, dimensions={0}, use_global_device_ids=true | all-gather | bytes 122880 | tf_op jit(solution)/shard_map/all_gather | solution.py:18
  54.6 0.1 convert_element_type.168
  54.7 11.9 %all_gather.16 = bf16[4,6,32]{2,1,0:T(8,128)(2,1)S(1)} all-gather(bf16[1,6,32]{2,1,0:T(8,128)(2,1)S(1)} %convert_element_type.168), channel_id=1, replica_groups=mesh['dp'=4,'kv'=4,'tp'=2] {'kv'}, dimensions={0}, use_global_device_ids=true | all-gather | bytes 1920 | tf_op jit(solution)/shard_map/all_gather | solution.py:18
  66.6 0.1 convert_element_type.164
  66.7 11.9 %all_gather.15 = bf16[4,6,32]{2,1,0:T(8,128)(2,1)S(1)} all-gather(bf16[1,6,32]{2,1,0:T(8,128)(2,1)S(1)} %convert_element_type.164), channel_id=1, replica_groups=mesh['dp'=4,'kv'=4,'tp'=2] {'kv'}, dimensions={0}, use_global_device_ids=true | all-gather | bytes 1920 | tf_op jit(solution)/shard_map/all_gather | solution.py:18
  78.6 1.3 while.19
  78.7 0.1 broadcast_in_dim.93
  78.8 0.1 reshape.164
  78.9 0.1 reshape.165
  79.2 0.1 reshape.164
  79.4 0.1 reshape.165
  79.6 0.1 reshape.164
  79.8 0.1 reshape.165
  80.0 0.1 reshape.161
  80.1 0.1 fusion.44
  80.2 0.1 mul.155
  80.3 0.1 broadcast_in_dim.71
  80.4 0.1 reshape.147
  80.5 0.1 broadcast_in_dim.72
  80.6 0.1 reshape.148
  80.8 0.1 reshape.150
  81.0 0.1 reshape.149
  81.1 2.8 %convolution_convert_fusion.2 = bf16[6,1024]{1,0:T(8,128)(2,1)S(1)} fusion(bf16[2048,1024]{1,0:T(8,128)(2,1)} %param.28, f32[6,2048]{1,0:T(8,128)S(1)} %reshape.150, f32[6,2048]{1,0:T(8,128)S(1)} %reshape.148, f32[6,2048]{1,0:T(8,128)S(1)} %reshape.149, f32[6,2048]{1,0:T(8,128)S(1)} %get-tuple-element.183, f32[6,2048]{1,0:T(8,128)S(1)} %reshape.147), kind=kOutput, calls=%fused_computation.16 | convolution fusion | flops 25233408 | bytes 4452352 | tf_op jit(solution)/shard_map/dot_general | solution.py:138
  83.9 3.4 %psum.47 = bf16[6,1024]{1,0:T(8,128)(2,1)S(1)} all-reduce(bf16[6,1024]{1,0:T(8,128)(2,1)S(1)} %convolution_convert_fusion.2), channel_id=1, replica_groups=mesh['dp'=4,'kv'=4,'tp'=2] {'tp'}, use_global_device_ids=true, to_apply=%region_10.11 | all-reduce | flops 6144 | bytes 24576 | tf_op jit(solution)/shard_map/psum | solution.py:139
  87.3 13.1 %all_gather.18 = bf16[6,4096]{1,0:T(8,128)(2,1)S(1)} all-gather(bf16[6,1024]{1,0:T(8,128)(2,1)S(1)} %fusion.21), channel_id=1, replica_groups=mesh['dp'=4,'kv'=4,'tp'=2] {'kv'}, dimensions={1}, use_global_device_ids=true | all-gather | bytes 61440 | tf_op jit(solution)/shard_map/all_gather | solution.py:141
  100.4 0.1 multiply_reduce_fusion
  100.6 12.9 %convolution_convert_fusion = bf16[6,4096]{1,0:T(8,128)(2,1)S(1)} fusion(bf16[2048,4096]{1,0:T(8,128)(2,1)} %param.31, bf16[4096,2048]{1,0:T(8,128)(2,1)} %param.30, f32[6]{0:T(128)S(1)} %add_rsqrt_fusion, f32[4096]{0:T(1024)S(1)} %copy-done.2, bf16[6,4096]{1,0:T(8,128)(2,1)S(1)} %all_gather.18), kind=kOutput, calls=%fused_computation.8 | convolution fusion | flops 201486336 | bytes 33669144 | tf_op jit(solution)/shard_map/dot_general | solution.py:151
  113.6 0.7 convert_element_type.190
  114.3 5.9 %reduce-scatter.3.cloned.1.call-done = bf16[6,2048]{1,0:T(8,128)(2,1)} async-done(((bf16[6,4096]{1,0:T(8,128)(2,1)}), bf16[6,2048]{1,0:T(8,128)(2,1)}) %reduce-scatter.3.cloned.1.call-update) | async-done | bytes 24592 | tf_op jit(solution)/shard_map/reduce_scatter | solution.py:160
  120.2 1.4 convert_element_type.191
  121.6 21.3 %reduce-scatter.5.cloned.1.call-done = f32[6,512]{1,0:T(8,128)} async-done(((f32[6,2048]{1,0:T(8,128)}), f32[6,512]{1,0:T(8,128)}) %reduce-scatter.5.cloned.1.call-update) | async-done | bytes 12304 | tf_op jit(solution)/shard_map/reduce_scatter | solution.py:163
  142.9 1.3 add_convert_fusion
  (39 shorter events, 1.1 us)
Async XLA Ops:
  6.5 3.8 %copy-start = (bf16[1024,128]{1,0:T(8,128)(2,1)S(1)}, bf16[1024,128]{1,0:T(8,128)(2,1)}, u32[]{:S(2)}) copy-start(bf16[1024,128]{1,0:T(8,128)(2,1)} %param.22) | copy-start | bytes 786436
  6.5 80.7 %copy-start.1 = (bf16[6,1024]{1,0:T(8,128)(2,1)S(1)}, bf16[6,1024]{1,0:T(8,128)(2,1)}, u32[]{:S(2)}) copy-start(bf16[6,1024]{1,0:T(8,128)(2,1)} %param.17) | copy-start | bytes 36868
  6.5 94.1 %copy-start.2 = (f32[4096]{0:T(1024)S(1)}, f32[4096]{0:T(1024)}, u32[]{:S(2)}) copy-start(f32[4096]{0:T(1024)} %param.29) | copy-start | bytes 49156
  6.5 113.7 %reduce-scatter.3.cloned.1.call-start = ((), (), s32[]{:S(2)}) async-start(), calls=%async_computation.2 | async-start | bytes 98304 | tf_op jit(solution)/shard_map/reduce_scatter | solution.py:160
  114.3 28.6 %reduce-scatter.5.cloned.1.call-start = ((), (), s32[]{:S(2)}) async-start(), calls=%async_computation.3 | async-start | bytes 81920 | tf_op jit(solution)/shard_map/reduce_scatter | solution.py:163
Sparse Core Ops, SparseCore 0:
  114.4 5.7 reduce-scatter.2
  122.5 20.4 reduce-scatter.4
where the time goes:
time: 152 us; the launch traced here: 151 us
  blocking collectives  76 us (50%)
  waiting for transfers between devices  27.2 us (18%)
  matrix products  22.9 us (15%)
  between operations  13.6 us (9%)
  other arithmetic  5.77 us (4%)
  local copies, waits for them, and re-layouts  5.52 us (4%)
    all_gather x3, blocking collectives, combined_all(): lax.all_gather(part.astype(kind), axis)  37.4 us
    psum x1, blocking collectives, shards(): lax.psum((query_part, key_part, value_part, forget_part, square_part), 'kv')  22.1 us
    reduce_scatter x1, waiting for transfers between devices, shards(): lax.psum_scatter(pair_share, 'kv', scatter_dimension=1, tiled=True)  21.3 us
    all_gather x1, blocking collectives, shards(): mid_rows = lax.all_gather(mid_cols, 'kv', axis=1, tiled=True)  13.1 us
    dot_general x1, matrix products, shards(): jnp.dot(hidden, down_weight, preferred_element_type=jnp.float32)  12.9 us
    reduce_scatter x1, waiting for transfers between devices, shards(): lax.psum_scatter(reordered.astype(jnp.bfloat16), 'tp', scatter_dimension=...  5.88 us
    psum x1, blocking collectives, shards(): lax.psum(partial_out.astype(jnp.bfloat16), 'tp').astype(jnp.float32)  3.36 us
  transfers between devices with their start and end apart: 2, of which 2 were waited for; matrix products, arithmetic and copies ran while one was open for 0% of the time, Pallas kernels for 0%

commit v1 on v0

--- a/solution.py
+++ b/solution.py
@@ -1,6 +1,10 @@
+import functools
+
 import jax
 import jax.numpy as jnp
 from jax import lax
+from jax.experimental import pallas as pl
+from jax.experimental.pallas import tpu as pltpu
 from jax.sharding import PartitionSpec as P
 
 D = 4096
@@ -43,7 +47,7 @@
     )
 
 
-def shards(
+def general_shards(
     tokens,
     lengths,
     attn_gain,
@@ -167,6 +171,496 @@
     return (mid_share + mixer_share).astype(jnp.bfloat16)
 
 
+BF = jnp.bfloat16
+F32 = jnp.float32
+PAD = 8
+LANES = 128
+MESH = pl.DeviceIdType.MESH
+
+
+def dot32(a, b):
+    return jnp.dot(a, b, preferred_element_type=F32)
+
+
+def layer_kernel(
+    kv_n,
+    tp_n,
+    lengths,
+    offset,
+    tokens_hbm,
+    gain_hbm,
+    wq_hbm,
+    wk_hbm,
+    wv_hbm,
+    fw_hbm,
+    ck_hbm,
+    cv_hbm,
+    gate_hbm,
+    wo_hbm,
+    mlp_hbm,
+    wu_hbm,
+    wd_hbm,
+    out_ref,
+    tok_all,
+    gain,
+    wq,
+    wk,
+    wv,
+    fw,
+    ck,
+    cv,
+    gate,
+    wo,
+    mlp,
+    wu,
+    wd,
+    rows32,
+    q_own,
+    q_send,
+    q_recv,
+    st_send,
+    st_recv,
+    q_heads,
+    val_send,
+    val_recv,
+    lse_send,
+    lse_recv,
+    att_heads,
+    part_recv,
+    mid,
+    hidden,
+    fin_send,
+    fin_recv,
+    load_sem,
+    up_sem,
+    down_sem,
+    tok_ss,
+    tok_rs,
+    q_ss,
+    q_rs,
+    st_ss,
+    st_rs,
+    val_ss,
+    val_rs,
+    lse_ss,
+    lse_rs,
+    part_ss,
+    part_rs,
+    fin_ss,
+    fin_rs,
+):
+    dp = lax.axis_index("dp")
+    z = lax.axis_index("kv")
+    t = lax.axis_index("tp")
+    n = kv_n * tp_n
+    rows, cols = tokens_hbm.shape
+    q_cols = wq.shape[1]
+    kv_cols = wk.shape[1]
+    here = ck.shape[1]
+    chunks = q_cols // LANES
+    half = LANES // 2
+
+    def peer(r):
+        dz, dt = r // tp_n, r % tp_n
+        return (dp, lax.rem(z + dz, kv_n), lax.rem(t + dt, tp_n))
+
+    barrier = pltpu.get_barrier_semaphore()
+    for r in range(1, n):
+        pl.semaphore_signal(barrier, inc=1, device_id=peer(r), device_id_type=MESH)
+
+    loads = {}
+
+    def load(name, source, target):
+        copy = pltpu.make_async_copy(source, target, load_sem.at[len(loads)])
+        copy.start()
+        loads[name] = copy
+
+    load("tokens", tokens_hbm, tok_all.at[z])
+    load("gain", gain_hbm, gain)
+    load("wq", wq_hbm, wq)
+    load("wk", wk_hbm, wk)
+    load("wv", wv_hbm, wv)
+    load("fw", fw_hbm, fw)
+    load("ck", ck_hbm, ck)
+    load("gate", gate_hbm, gate)
+    load("cv", cv_hbm, cv)
+    load("wo0", wo_hbm.at[0], wo.at[:, 0])
+    load("wo1", wo_hbm.at[1], wo.at[:, 1])
+    load("mlp", mlp_hbm, mlp)
+
+    up_tile = hidden.shape[1] // up_sem.shape[0]
+
+    def up_copy(j):
+        span = pl.ds(pl.multiple_of(j * up_tile, LANES), up_tile)
+        return pltpu.make_async_copy(wu_hbm.at[:, span], wu.at[:, span], up_sem.at[j])
+
+    def down_span(r):
+        _, pz, pt = peer(r)
+        width = fin_send.shape[2]
+        return pl.ds(pl.multiple_of((pz * tp_n + pt) * width, LANES), width)
+
+    def down_copy(r):
+        span = down_span(r)
+        return pltpu.make_async_copy(wd_hbm.at[:, span], wd.at[:, span], down_sem.at[r])
+
+    for j in range(up_sem.shape[0]):
+        up_copy(j).start()
+    for r in reversed(range(n)):
+        down_copy(r).start()
+
+    def send(source, target, ss, rs, r):
+        copy = pltpu.make_async_remote_copy(
+            src_ref=source,
+            dst_ref=target,
+            send_sem=ss,
+            recv_sem=rs,
+            device_id=peer(r),
+            device_id_type=MESH,
+        )
+        copy.start()
+        return copy
+
+    rows32[...] = jnp.zeros_like(rows32)
+    loads["tokens"].wait()
+    loads["gain"].wait()
+    rows32[0:rows, :] = tok_all[z].astype(F32)
+    own_rows = rows32[...]
+    scaled = (own_rows * gain[...]).astype(BF)
+    scaled32 = scaled.astype(F32)
+    loads["fw"].wait()
+    fw_here = fw[:, pl.ds(pl.multiple_of(z * cols, LANES), cols)].astype(F32)
+    lane = lax.broadcasted_iota(jnp.int32, (PAD, LANES), 1)
+    stats = jnp.where(
+        lane == KEY_VALUE_HEADS, jnp.sum(own_rows * own_rows, axis=1, keepdims=True), 0.0
+    )
+    for h in range(KEY_VALUE_HEADS):
+        part = jnp.sum(scaled32 * fw_here[h : h + 1, :], axis=1, keepdims=True)
+        stats = jnp.where(lane == h, part, stats)
+    st_send[...] = stats
+
+    loads["wq"].wait()
+    q_tile = 512 if q_cols % 512 == 0 else LANES
+
+    @pl.loop(0, q_cols // q_tile)
+    def _(j):
+        span = pl.ds(pl.multiple_of(j * q_tile, LANES), q_tile)
+        part = dot32(scaled, wq[:, span])
+        q_own[:, span] = part
+        q_send[:, span] = part.astype(BF)
+
+    loads["wk"].wait()
+    loads["wv"].wait()
+    for place, weight in ((q_cols, wk), (q_cols + kv_cols, wv)):
+        part = dot32(scaled, weight[...])
+        q_own[:, place : place + kv_cols] = part
+        q_send[:, place : place + kv_cols] = part.astype(BF)
+
+    pl.semaphore_wait(barrier, n - 1)
+    sent = []
+    q_copies, val_copies = [], []
+    for dz in reversed(range(1, kv_n)):
+        r = dz * tp_n
+        k = dz - 1
+        q_copies.append(send(q_send, q_recv.at[k], q_ss.at[k], q_rs.at[k], r))
+        q_copies.append(send(st_send, st_recv.at[k], st_ss.at[k], st_rs.at[k], r))
+    tok_copies = []
+    for dz in range(1, kv_n):
+        k = dz - 1
+        tok_copies.append(
+            send(tok_all.at[z], tok_all.at[z], tok_ss.at[k], tok_rs.at[k], dz * tp_n)
+        )
+    for copy in q_copies:
+        copy.wait_recv()
+    q_sum = q_own[...]
+    st_sum = st_send[...]
+    for k in range(kv_n - 1):
+        q_sum = q_sum + q_recv[k].astype(F32)
+        st_sum = st_sum + st_recv[k]
+    square = st_sum[:, KEY_VALUE_HEADS : KEY_VALUE_HEADS + 1]
+    row_scale = lax.rsqrt(square / (cols * kv_n) + epsilon)
+    q_sum = (q_sum * row_scale).astype(BF).astype(F32)
+    for c in range(chunks):
+        q_heads[c] = q_sum[:, c * LANES : (c + 1) * LANES]
+    new_key = q_sum[:, q_cols : q_cols + kv_cols]
+    new_value = q_sum[:, q_cols + kv_cols :]
+    local = KEY_VALUE_HEADS // tp_n
+    forgets = []
+    for g in range(local):
+        raw = st_sum[:, g : g + 1]
+        for other in range(1, tp_n):
+            at = other * local + g
+            raw = jnp.where(t == other, st_sum[:, at : at + 1], raw)
+        x = raw * row_scale + offset[g]
+        forgets.append(jnp.minimum(x, 0.0) - jnp.log(1.0 + jnp.exp(-jnp.abs(x))))
+
+    scale = HD ** (-0.5)
+    low8 = lax.broadcasted_iota(jnp.int32, (chunks // 2, LANES), 1) < half
+    lane16 = lax.broadcasted_iota(jnp.int32, (chunks, LANES), 1)
+    low16 = lane16 < half
+    position = z * here + lax.broadcasted_iota(jnp.int32, (2 * chunks, here), 1)
+    loads["ck"].wait()
+    loads["gate"].wait()
+    loads["cv"].wait()
+    lse_all = jnp.zeros((chunks, LANES), F32)
+    own_scores, own_lse, own_vals = [], [], []
+    hc = chunks // 2
+    for b in range(rows):
+        x = q_heads[:, b, :]
+        turned = pltpu.roll(x, half, 1)
+        spread = jnp.concatenate(
+            [
+                jnp.where(low8, x[:hc], 0.0),
+                jnp.where(low8, turned[:hc], 0.0),
+                jnp.where(low8, 0.0, turned[hc:]),
+                jnp.where(low8, 0.0, x[hc:]),
+            ],
+            axis=0,
+        )
+        own = jnp.sum(spread * new_key[b : b + 1, :], axis=1, keepdims=True) * scale
+        own_scores.append(jnp.where(low16, own[:chunks], own[chunks:]))
+        scores = scale * lax.dot_general(
+            spread.astype(BF), ck[b], (((1,), (1,)), ((), ())), preferred_element_type=F32
+        )
+        bias = jnp.concatenate(
+            [
+                jnp.broadcast_to(gate[b, g : g + 1, :] + forgets[g][b : b + 1, :], (chunks, here))
+                for g in range(local)
+            ],
+            axis=0,
+        )
+        live = position < lengths[b]
+        scores = jnp.where(live, scores + bias, floor_score)
+        top = jnp.max(scores, axis=1, keepdims=True)
+        weights = jnp.where(live, jnp.exp(scores - top), 0.0)
+        total = jnp.maximum(jnp.sum(weights, axis=1, keepdims=True), 1e-30)
+        vals = dot32(weights.astype(BF), cv[b]) / total
+        lse = top + jnp.log(total)
+        lse = jnp.where(low16, lse[:chunks], lse[chunks:])
+        vals = jnp.where(low16, vals[:chunks], vals[chunks:])
+        own_lse.append(lse)
+        own_vals.append(vals)
+        lse_all = jnp.where((lane16 & (half - 1)) == b, lse, lse_all)
+        val_send[b * chunks : (b + 1) * chunks, :] = vals.astype(BF)
+    lse_send[...] = lse_all
+    for dz in reversed(range(1, kv_n)):
+        r = dz * tp_n
+        k = dz - 1
+        val_copies.append(send(val_send, val_recv.at[k], val_ss.at[k], val_rs.at[k], r))
+        val_copies.append(send(lse_send, lse_recv.at[k], lse_ss.at[k], lse_rs.at[k], r))
+    att_heads[...] = jnp.zeros_like(att_heads)
+    for copy in val_copies:
+        copy.wait_recv()
+    for b in range(rows):
+        levels = [own_scores[b], own_lse[b]]
+        terms = [jnp.broadcast_to(new_value[b : b + 1, :], (chunks, LANES)), own_vals[b]]
+        for k in range(kv_n - 1):
+            got = lse_recv[k]
+            levels.append(
+                jnp.where(low16, got[:, b : b + 1], got[:, half + b : half + b + 1])
+            )
+            terms.append(val_recv[k, b * chunks : (b + 1) * chunks, :].astype(F32))
+        peak = functools.reduce(jnp.maximum, levels)
+        bottom = jnp.zeros((chunks, LANES), F32)
+        upper = jnp.zeros((chunks, LANES), F32)
+        for level, term in zip(levels, terms):
+            share = jnp.exp(level - peak)
+            bottom = bottom + share
+            upper = upper + share * term
+        att_heads[:, b, :] = upper / bottom
+
+    order = [c // 2 + (c % 2) * hc for c in range(chunks)]
+    attended = jnp.concatenate([att_heads[c] for c in order], axis=1).astype(BF)
+    loads["wo0"].wait()
+    loads["wo1"].wait()
+    o_tile = 256 if cols % 256 == 0 else LANES
+    for j in range(cols // o_tile):
+        weight = wo[:, :, :, j * o_tile : (j + 1) * o_tile].reshape(q_cols, o_tile)
+        part_recv[z, t, :, j * o_tile : (j + 1) * o_tile] = dot32(attended, weight).astype(BF)
+    part_copies = []
+    for r in reversed(range(1, n)):
+        part_copies.append(
+            send(part_recv.at[z, t], part_recv.at[z, t], part_ss.at[r], part_rs.at[r], r)
+        )
+    for copy in tok_copies:
+        copy.wait_recv()
+    for copy in part_copies:
+        copy.wait_recv()
+    mid[...] = jnp.zeros_like(mid)
+    for s in range(kv_n):
+        mid[0:rows, s * cols : (s + 1) * cols] = tok_all[s].astype(F32)
+    for s in range(kv_n):
+        span = slice(s * cols, (s + 1) * cols)
+        total = mid[:, span]
+        for g in range(tp_n):
+            total = total + part_recv[s, g].astype(F32)
+        mid[:, span] = total.astype(BF).astype(F32)
+
+    wide = mid[...]
+    loads["mlp"].wait()
+    inverse = lax.rsqrt(jnp.mean(wide * wide, axis=1, keepdims=True) + epsilon)
+    normed = (wide * mlp[...] * inverse).astype(BF)
+
+    @pl.loop(0, up_sem.shape[0])
+    def _(j):
+        up_copy(j).wait()
+        span = pl.ds(pl.multiple_of(j * up_tile, LANES), up_tile)
+        hot = jnp.maximum(dot32(normed, wu[:, span]), 0.0)
+        hidden[:, span] = (hot * hot).astype(BF)
+
+    def fin_copy(r):
+        return pltpu.make_async_remote_copy(
+            src_ref=fin_send.at[r],
+            dst_ref=fin_recv.at[r],
+            send_sem=fin_ss.at[r],
+            recv_sem=fin_rs.at[r],
+            device_id=peer(r),
+            device_id_type=MESH,
+        )
+
+    active = hidden[...]
+
+    @pl.loop(0, n - 1)
+    def _(i):
+        r = n - 1 - i
+        down_copy(r).wait()
+        fin_send[r] = dot32(active, wd[:, down_span(r)]).astype(BF)
+        fin_copy(r).start()
+
+    down_copy(0).wait()
+    result = dot32(active, wd[:, down_span(0)]) + mid[:, down_span(0)]
+    for r in reversed(range(1, n)):
+        fin_copy(r).wait_recv()
+        result = result + fin_recv[r].astype(F32)
+    out_ref[...] = result[0:rows, :].astype(BF)
+    for copy in q_copies + tok_copies + val_copies + part_copies:
+        copy.wait_send()
+    for r in range(1, n):
+        fin_copy(r).wait_send()
+
+
+def kernel_shards(
+    kv_n,
+    tp_n,
+    tokens,
+    lengths,
+    attn_gain,
+    query_weight,
+    key_weight,
+    value_weight,
+    forget_weight,
+    forget_offset,
+    cache_keys,
+    cache_values,
+    gate_sum,
+    out_weight,
+    mlp_gain,
+    up_weight,
+    down_weight,
+):
+    rows, cols = tokens.shape
+    n = kv_n * tp_n
+    q_cols = query_weight.shape[1]
+    kv_cols = key_weight.shape[1]
+    chunks = q_cols // LANES
+    local = kv_cols // HD
+    units = up_weight.shape[1]
+    width = down_weight.shape[1]
+    out_cols = width // n
+    out_blocks = out_weight.reshape(local, chunks, HD, cols)
+    up_tiles = 4
+    peers = kv_n - 1
+    vm = pltpu.VMEM
+    dma = pltpu.SemaphoreType.DMA
+    any_spec = pl.BlockSpec(memory_space=pl.ANY)
+    smem_spec = pl.BlockSpec(memory_space=pltpu.SMEM)
+    moved = (
+        tokens,
+        attn_gain.reshape(1, cols),
+        query_weight,
+        key_weight,
+        value_weight,
+        forget_weight.T,
+        cache_keys,
+        cache_values,
+        gate_sum,
+        out_blocks,
+        mlp_gain.reshape(1, width),
+        up_weight,
+        down_weight,
+    )
+    scratch = [
+        vm((kv_n, rows, cols), BF),
+        vm((1, cols), F32),
+        vm(query_weight.shape, BF),
+        vm(key_weight.shape, BF),
+        vm(value_weight.shape, BF),
+        vm(forget_weight.shape[::-1], BF),
+        vm(cache_keys.shape, BF),
+        vm(cache_values.shape, BF),
+        vm(gate_sum.shape, F32),
+        vm((chunks, local, HD, cols), BF),
+        vm((1, width), F32),
+        vm(up_weight.shape, BF),
+        vm(down_weight.shape, BF),
+        vm((PAD, cols), F32),
+        vm((PAD, q_cols + 2 * kv_cols), F32),
+        vm((PAD, q_cols + 2 * kv_cols), BF),
+        vm((peers, PAD, q_cols + 2 * kv_cols), BF),
+        vm((PAD, LANES), F32),
+        vm((peers, PAD, LANES), F32),
+        vm((chunks, PAD, LANES), F32),
+        vm((rows * chunks, LANES), BF),
+        vm((peers, rows * chunks, LANES), BF),
+        vm((chunks, LANES), F32),
+        vm((peers, chunks, LANES), F32),
+        vm((chunks, PAD, LANES), F32),
+        vm((kv_n, tp_n, PAD, cols), BF),
+        vm((PAD, width), F32),
+        vm((PAD, units), BF),
+        vm((n, PAD, out_cols), BF),
+        vm((n, PAD, out_cols), BF),
+        dma((12,)),
+        dma((up_tiles,)),
+        dma((n,)),
+    ]
+    for count in (peers, peers, peers, peers, peers, n, n):
+        scratch += [dma((count,)), dma((count,))]
+    return pl.pallas_call(
+        functools.partial(layer_kernel, kv_n, tp_n),
+        out_shape=jax.ShapeDtypeStruct((rows, out_cols), BF),
+        in_specs=[smem_spec] * 2 + [any_spec] * len(moved),
+        out_specs=pl.BlockSpec(memory_space=pltpu.VMEM),
+        scratch_shapes=scratch,
+        compiler_params=pltpu.CompilerParams(
+            collective_id=0, has_side_effects=True, vmem_limit_bytes=60 * 1024 * 1024
+        ),
+        name="layer",
+    )(lengths, forget_offset, *moved)
+
+
+def fits(kv_n, tp_n, tokens, query_weight, key_weight, forget_weight, up_weight, down_weight):
+    rows, cols = tokens.shape
+    held = 4 * query_weight.size + up_weight.size * 2 + down_weight.size * 2
+    return (
+        rows <= PAD
+        and kv_n > 1
+        and cols % LANES == 0
+        and key_weight.shape[1] == LANES
+        and HD * 2 == LANES
+        and up_weight.shape[1] % (4 * LANES) == 0
+        and down_weight.shape[1] % (kv_n * tp_n * LANES) == 0
+        and held < 48 * 1024 * 1024
+    )
+
+
+def shards(*args):
+    kv_n = lax.axis_size("kv")
+    tp_n = lax.axis_size("tp")
+    if fits(kv_n, tp_n, args[0], args[3], args[4], args[6], args[13], args[14]):
+        return kernel_shards(kv_n, tp_n, *args)
+    return general_shards(*args)
+
+
 def solution(mesh):
     placed = (
         P("dp", "kv"),

time: 152 us -> 35.9 us (0.24)
  blocking collectives: 76 us -> 0 us
  Pallas kernels: 0 us -> 34.2 us
  waiting for transfers between devices: 27.2 us -> 0 us
  matrix products: 22.9 us -> 0 us
  between operations: 13.6 us -> 0.01 us
  other arithmetic: 5.77 us -> 0 us
  local copies, waits for them, and re-layouts: 5.52 us -> 1.3 us
    all_gather x4 -> x0, blocking collectives: 50.6 us -> none  [the longest x3 37.4 us: combined_all(): lax.all_gather(part.astype(kind), axis)]
    pallas_call x0 -> x1, Pallas kernels: none -> 34.2 us  [kernel_shards(): pl.pallas_call(functools.partial(layer_kernel, kv_n, tp_n), out_shape=jax...]
    reduce_scatter x2 -> x0, waiting for transfers between devices: 27.1 us -> none  [the longest x1 21.3 us: shards(): lax.psum_scatter(pair_share, 'kv', scatter_dimension=1, tiled=True)]
    psum x2 -> x0, blocking collectives: 25.4 us -> none  [the longest x1 22.1 us: shards(): lax.psum((query_part, key_part, value_part, forget_part, square_part), 'kv')]
    dot_general x9 -> x0, matrix products: 22.9 us -> none  [the longest x1 12.9 us: shards(): jnp.dot(hidden, down_weight, preferred_element_type=jnp.float32)]
    convert_element_type x9 -> x0, other arithmetic: 2.81 us -> none  [the longest x1 1.38 us: shards(): pair_share = lax.psum_scatter(reordered.astype(jnp.bfloat16), 'tp', scatt...]
  transfers between devices with their start and end apart: 2 -> 0, of which waited for: 2 -> 0; matrix products, arithmetic and copies ran while one was open for 0% -> 0% of each run, Pallas kernels for 0% -> 0%
where the time goes in v1:
time: 35.9 us; the launch traced here: 35.5 us
  Pallas kernels  34.2 us (95%)
  local copies, waits for them, and re-layouts  1.3 us (4%)
    pallas_call x1, Pallas kernels, kernel_shards(): pl.pallas_call(functools.partial(layer_kernel, kv_n, tp_n), out_shape=jax...  34.2 us
    unnamed x1, local copies, waits for them, and re-layouts  1.3 us

profile of v1, /device:TPU:0, one launch (start us, length us, event | category | flops | bytes accessed | tf_op | source)
XLA Modules:
  0.0 35.5 jit_solution(10128971780230658061)
XLA Ops:
  0.0 34.2 %layer.1 = bf16[6,512]{1,0:T(8,128)(2,1)} custom-call(s32[6]{0:T(128)} %lengths.1, f32[2]{0:T(128)} %offset.1, bf16[6,1024]{1,0:T(8,128)(2,1)} %tokens_hbm.1, f32[1,1024]{1,0:T(1,128)} %bitcast.7, bf16[1024,2048]{1,0:T(8,128)(2,1)} %wq_hbm.1, bf16[1024,128]{1,0:T(8,128)(2,1)} %wk_hbm.1, bf16[1024,128]{1,0:T(8,128)(2,1)} %wv_hbm.1, bf16[4,4096]{1,0:T(4,128)(2,1)} %bitcast.5, ...), custom_call_target="tpu_custom_call" | custom-call | tf_op jit(solution)/shard_map/layer/pallas_call | solution.py:628
  34.2 1.3 %copy.17 = bf16[6,512]{1,0:T(8,128)(2,1)} copy(bf16[6,512]{1,0:T(8,128)(2,1)} %layer.1) | data formatting | bytes 12288

commit v2 on v1

--- a/solution.py
+++ b/solution.py
@@ -201,7 +201,7 @@
     wu_hbm,
     wd_hbm,
     out_ref,
-    tok_all,
+    tok_in,
     gain,
     wq,
     wk,
@@ -234,8 +234,6 @@
     load_sem,
     up_sem,
     down_sem,
-    tok_ss,
-    tok_rs,
     q_ss,
     q_rs,
     st_ss,
@@ -275,12 +273,15 @@
         copy.start()
         loads[name] = copy
 
-    load("tokens", tokens_hbm, tok_all.at[z])
+    load("tokens", tokens_hbm, tok_in)
     load("gain", gain_hbm, gain)
-    load("wq", wq_hbm, wq)
+    load("fw", fw_hbm, fw)
+    q_pieces = q_ss.shape[0]
+    piece = q_cols // q_pieces
+    for j in range(q_pieces):
+        load(f"wq{j}", wq_hbm.at[:, pl.ds(j * piece, piece)], wq.at[:, pl.ds(j * piece, piece)])
     load("wk", wk_hbm, wk)
     load("wv", wv_hbm, wv)
-    load("fw", fw_hbm, fw)
     load("ck", ck_hbm, ck)
     load("gate", gate_hbm, gate)
     load("cv", cv_hbm, cv)
@@ -323,7 +324,7 @@
     rows32[...] = jnp.zeros_like(rows32)
     loads["tokens"].wait()
     loads["gain"].wait()
-    rows32[0:rows, :] = tok_all[z].astype(F32)
+    rows32[0:rows, :] = tok_in[...].astype(F32)
     own_rows = rows32[...]
     scaled = (own_rows * gain[...]).astype(BF)
     scaled32 = scaled.astype(F32)
@@ -338,37 +339,39 @@
         stats = jnp.where(lane == h, part, stats)
     st_send[...] = stats
 
-    loads["wq"].wait()
-    q_tile = 512 if q_cols % 512 == 0 else LANES
-
-    @pl.loop(0, q_cols // q_tile)
-    def _(j):
-        span = pl.ds(pl.multiple_of(j * q_tile, LANES), q_tile)
+    q_copies, val_copies = [], []
+    for j in range(q_pieces):
+        loads[f"wq{j}"].wait()
+        span = pl.ds(j * piece, piece)
         part = dot32(scaled, wq[:, span])
         q_own[:, span] = part
         q_send[:, span] = part.astype(BF)
-
-    loads["wk"].wait()
-    loads["wv"].wait()
-    for place, weight in ((q_cols, wk), (q_cols + kv_cols, wv)):
-        part = dot32(scaled, weight[...])
-        q_own[:, place : place + kv_cols] = part
-        q_send[:, place : place + kv_cols] = part.astype(BF)
-
-    pl.semaphore_wait(barrier, n - 1)
-    sent = []
-    q_copies, val_copies = [], []
-    for dz in reversed(range(1, kv_n)):
-        r = dz * tp_n
-        k = dz - 1
-        q_copies.append(send(q_send, q_recv.at[k], q_ss.at[k], q_rs.at[k], r))
-        q_copies.append(send(st_send, st_recv.at[k], st_ss.at[k], st_rs.at[k], r))
-    tok_copies = []
-    for dz in range(1, kv_n):
-        k = dz - 1
-        tok_copies.append(
-            send(tok_all.at[z], tok_all.at[z], tok_ss.at[k], tok_rs.at[k], dz * tp_n)
-        )
+        if j == q_pieces - 1:
+            loads["wk"].wait()
+            loads["wv"].wait()
+            for place, weight in ((q_cols, wk), (q_cols + kv_cols, wv)):
+                part = dot32(scaled, weight[...])
+                q_own[:, place : place + kv_cols] = part
+                q_send[:, place : place + kv_cols] = part.astype(BF)
+            span = pl.ds(j * piece, piece + 2 * kv_cols)
+        if j == 0:
+            pl.semaphore_wait(barrier, n - 1)
+            for dz in reversed(range(1, kv_n)):
+                k = dz - 1
+                q_copies.append(
+                    send(st_send, st_recv.at[k], st_ss.at[k], st_rs.at[k], dz * tp_n)
+                )
+        for dz in reversed(range(1, kv_n)):
+            k = dz - 1
+            q_copies.append(
+                send(
+                    q_send.at[:, span],
+                    q_recv.at[k, :, span],
+                    q_ss.at[j, k],
+                    q_rs.at[j, k],
+                    dz * tp_n,
+                )
+            )
     for copy in q_copies:
         copy.wait_recv()
     q_sum = q_own[...]
@@ -472,28 +475,24 @@
     attended = jnp.concatenate([att_heads[c] for c in order], axis=1).astype(BF)
     loads["wo0"].wait()
     loads["wo1"].wait()
+    residual = jnp.where(t == 0, rows32[...], 0.0)
     o_tile = 256 if cols % 256 == 0 else LANES
     for j in range(cols // o_tile):
         weight = wo[:, :, :, j * o_tile : (j + 1) * o_tile].reshape(q_cols, o_tile)
-        part_recv[z, t, :, j * o_tile : (j + 1) * o_tile] = dot32(attended, weight).astype(BF)
+        share = dot32(attended, weight) + residual[:, j * o_tile : (j + 1) * o_tile]
+        part_recv[z, t, :, j * o_tile : (j + 1) * o_tile] = share.astype(BF)
     part_copies = []
     for r in reversed(range(1, n)):
         part_copies.append(
             send(part_recv.at[z, t], part_recv.at[z, t], part_ss.at[r], part_rs.at[r], r)
         )
-    for copy in tok_copies:
-        copy.wait_recv()
     for copy in part_copies:
         copy.wait_recv()
-    mid[...] = jnp.zeros_like(mid)
     for s in range(kv_n):
-        mid[0:rows, s * cols : (s + 1) * cols] = tok_all[s].astype(F32)
-    for s in range(kv_n):
-        span = slice(s * cols, (s + 1) * cols)
-        total = mid[:, span]
-        for g in range(tp_n):
+        total = part_recv[s, 0].astype(F32)
+        for g in range(1, tp_n):
             total = total + part_recv[s, g].astype(F32)
-        mid[:, span] = total.astype(BF).astype(F32)
+        mid[:, s * cols : (s + 1) * cols] = total.astype(BF).astype(F32)
 
     wide = mid[...]
     loads["mlp"].wait()
@@ -532,7 +531,7 @@
         fin_copy(r).wait_recv()
         result = result + fin_recv[r].astype(F32)
     out_ref[...] = result[0:rows, :].astype(BF)
-    for copy in q_copies + tok_copies + val_copies + part_copies:
+    for copy in q_copies + val_copies + part_copies:
         copy.wait_send()
     for r in range(1, n):
         fin_copy(r).wait_send()
@@ -568,6 +567,7 @@
     out_cols = width // n
     out_blocks = out_weight.reshape(local, chunks, HD, cols)
     up_tiles = 4
+    pieces = 2 if q_cols % (2 * LANES) == 0 else 1
     peers = kv_n - 1
     vm = pltpu.VMEM
     dma = pltpu.SemaphoreType.DMA
@@ -589,7 +589,7 @@
         down_weight,
     )
     scratch = [
-        vm((kv_n, rows, cols), BF),
+        vm((rows, cols), BF),
         vm((1, cols), F32),
         vm(query_weight.shape, BF),
         vm(key_weight.shape, BF),
@@ -619,12 +619,12 @@
         vm((PAD, units), BF),
         vm((n, PAD, out_cols), BF),
         vm((n, PAD, out_cols), BF),
-        dma((12,)),
+        dma((11 + pieces,)),
         dma((up_tiles,)),
         dma((n,)),
     ]
-    for count in (peers, peers, peers, peers, peers, n, n):
-        scratch += [dma((count,)), dma((count,))]
+    for count in ((pieces, peers), (peers,), (peers,), (peers,), (n,), (n,)):
+        scratch += [dma(count), dma(count)]
     return pl.pallas_call(
         functools.partial(layer_kernel, kv_n, tp_n),
         out_shape=jax.ShapeDtypeStruct((rows, out_cols), BF),

time: 35.9 us -> 33.8 us (0.942)
  Pallas kernels: 34.2 us -> 32.2 us
    pallas_call x1, Pallas kernels: 34.2 us -> 32.2 us  [kernel_shards(): pl.pallas_call(functools.partial(layer_kernel, kv_n, tp_n), out_shape=jax...]
where the time goes in v2:
time: 33.8 us; the launch traced here: 33.5 us
  Pallas kernels  32.2 us (95%)
  local copies, waits for them, and re-layouts  1.3 us (4%)
    pallas_call x1, Pallas kernels, kernel_shards(): pl.pallas_call(functools.partial(layer_kernel, kv_n, tp_n), out_shape=jax...  32.2 us
    unnamed x1, local copies, waits for them, and re-layouts  1.3 us

profile of v2, /device:TPU:0, one launch (start us, length us, event | category | flops | bytes accessed | tf_op | source)
XLA Modules:
  0.0 33.5 jit_solution(12033917835651155887)
XLA Ops:
  0.0 32.2 %layer.1 = bf16[6,512]{1,0:T(8,128)(2,1)} custom-call(s32[6]{0:T(128)} %lengths.1, f32[2]{0:T(128)} %offset.1, bf16[6,1024]{1,0:T(8,128)(2,1)} %tokens_hbm.1, f32[1,1024]{1,0:T(1,128)} %bitcast.7, bf16[1024,2048]{1,0:T(8,128)(2,1)} %wq_hbm.1, bf16[1024,128]{1,0:T(8,128)(2,1)} %wk_hbm.1, bf16[1024,128]{1,0:T(8,128)(2,1)} %wv_hbm.1, bf16[4,4096]{1,0:T(4,128)(2,1)} %bitcast.5, ...), custom_call_target="tpu_custom_call" | custom-call | tf_op jit(solution)/shard_map/layer/pallas_call | solution.py:628
  32.2 1.3 %copy.17 = bf16[6,512]{1,0:T(8,128)(2,1)} copy(bf16[6,512]{1,0:T(8,128)(2,1)} %layer.1) | data formatting | bytes 12288
